TPU v7x, 32 devices: a whole 2x2x4 slice. The times are simulated.
32 devices in a mesh: sp: 8 (over z, y), tp: 4 (over x, core).
Axes of the slice: x: 2, y: 2, z: 4, core: 2. Of those that a mesh axis runs over, the one named last changes fastest.
Arguments:
- skip_stream: bfloat16 [6144, 2048], P(('sp', 'tp')), may hold values from -24 to 24
- acceptance_signal: bfloat16 [6144, 2048], P('sp', 'tp'), may hold values from -6 to 6
- lookup_mapped: bfloat16 [6144, 2048], P('sp', 'tp'), may hold values from -12 to 12
- payload_mapped: bfloat16 [6144, 2048], P('sp', 'tp'), may hold values from -6 to 6
- result_switch: bfloat16 [6144, 2048], P('sp', 'tp'), may hold values from -6 to 6
- forget_dynamic_share: bfloat16 [6144, 2048], P('sp', 'tp'), may hold values from -4 to 4
- additive_forget_logarithm: float32 [6144, 32], P('sp', 'tp'), may hold values from -1 to 0
- forget_feature_offset: float32 [2048], P('tp'), may hold values from -11 to -3
- substitution_dynamic_share: bfloat16 [6144, 2048], P('sp', 'tp'), may hold values from -6 to 6
- substitution_feature_offset: float32 [2048], P('tp'), may hold values from -6.5 to 2.5
- diagonal_reward_scales: float32 [2048], P('tp'), may hold values from -0.9 to 0.9
- result_matrix: bfloat16 [2048, 2048], P('tp'), may hold values from -0.125 to 0.125
- mlp_rescaler: float32 [2048], replicated, may hold values from 0.1 to 1.9
- switch_matrix: bfloat16 [2048, 5120], P('sp', 'tp'), may hold values from -0.125 to 0.125
- expand_matrix: bfloat16 [2048, 5120], P('sp', 'tp'), may hold values from -0.125 to 0.125
- contract_matrix: bfloat16 [2048, 5120], P('sp', 'tp'), may hold values from -0.25 to 0.25
Outputs:
- mixed_out: bfloat16 [6144, 2048], P(('sp', 'tp'))
All inputs are finite; a program needn't handle non-finite values.
Results may differ from a plain program's by a relative error of at most 0.015.
Values may be sent and summed in bfloat16 or wider, within the bound.
No kernel may reach another device: no remote copies, remote signals or barrier semaphores. Data moves between devices by JAX's collectives and lax.ppermute only.
A program may use at most 128 MiB of HBM per device.

v0:
```python
import jax
import jax.numpy as jnp
from jax import lax
from jax.sharding import PartitionSpec as P

PER_GROUP_DIMS = 64


norm_eps = 1e-06
group_eps = 0.00064
half_step = 0.5
exact = lax.Precision.HIGHEST


def prefix(shard, axis, join, neutral):
    place = lax.axis_index(axis)
    gathered = jax.tree.map(
        lambda a, kind: lax.all_gather(a.astype(kind), axis), shard, (jnp.bfloat16, jnp.bfloat16)
    )
    state = jax.tree.map(lambda a, e: jnp.zeros_like(a) + jnp.asarray(e, a.dtype), shard, neutral)

    def one(turn, state):
        return join(
            state,
            jax.tree.map(
                lambda a, own: lax.dynamic_index_in_dim(a, turn, 0, False).astype(own.dtype),
                gathered,
                shard,
            ),
        )

    return lax.fori_loop(0, place, one, state)


def compose(earlier, latter):
    prod_first, carry_first = earlier
    prod_second, carry_second = latter
    product = jnp.einsum("hij,hjk->hik", prod_first, prod_second, precision=exact)
    carried = jnp.einsum("hij,hjk->hik", carry_first, prod_second, precision=exact) + carry_second
    return (product, carried)


def masked_pairs(left, right, keep):
    return jnp.where(keep, jnp.einsum("htc,hjc->htj", left, right, precision=exact), 0.0)


def block_step(carry, inputs):
    state_part, transition = carry
    read_blk, logstep_blk, key_blk, value_blk, unit_blk, rate_blk = inputs
    length = read_blk.shape[1]
    width = value_blk.shape[2]
    cumulate = jnp.cumsum(logstep_blk, axis=1)
    growth = jnp.exp(cumulate)
    shrink = jnp.exp(-cumulate)
    before_unit = jnp.exp(cumulate - logstep_blk) * unit_blk
    erase_dir = unit_blk * rate_blk
    key_back = key_blk * shrink
    erase_back = erase_dir * shrink
    read_fwd = read_blk * growth
    end_growth = growth[:, -1:, :]
    key_end = key_back * end_growth
    erase_end = erase_back * end_growth
    row_index = lax.broadcasted_iota(jnp.int32, (length, length), 0)
    col_index = lax.broadcasted_iota(jnp.int32, (length, length), 1)
    strict = col_index < row_index
    inclusive = col_index <= row_index
    key_past = masked_pairs(before_unit, key_back, strict)
    erase_past = masked_pairs(before_unit, erase_back, strict)
    key_read = masked_pairs(read_fwd, key_back, inclusive)
    erase_read = masked_pairs(read_fwd, erase_back, inclusive)
    recall_rhs = jnp.einsum("htk,hvk->htv", before_unit, state_part, precision=exact) + jnp.einsum(
        "htj,hjv->htv", key_past, value_blk, precision=exact
    )
    solved = jax.scipy.linalg.solve_triangular(
        erase_past,
        jnp.concatenate([recall_rhs, before_unit], axis=-1),
        lower=True,
        unit_diagonal=True,
    )
    recalled = solved[..., :width]
    carried_map = solved[..., width:]
    local_out = (
        jnp.einsum("htk,hvk->htv", read_fwd, state_part, precision=exact)
        + jnp.einsum("htj,hjv->htv", key_read, value_blk, precision=exact)
        - jnp.einsum("htj,hjv->htv", erase_read, recalled, precision=exact)
    )
    from_start = read_fwd - jnp.einsum("htj,hjk->htk", erase_read, carried_map, precision=exact)
    coefficient = jnp.einsum("htk,hjk->htj", from_start, transition, precision=exact)
    new_state = (
        state_part * end_growth
        + jnp.einsum("htv,htk->hvk", value_blk, key_end, precision=exact)
        - jnp.einsum("htv,htk->hvk", recalled, erase_end, precision=exact)
    )
    step_map = jnp.eye(width, dtype=jnp.float32)[None] * end_growth - jnp.einsum(
        "htj,htk->hjk", carried_map, erase_end, precision=exact
    )
    new_transition = jnp.einsum("hij,hjk->hik", transition, step_map, precision=exact)
    return ((new_state, new_transition), (local_out, coefficient))


def per_device(
    skip_stream,
    acceptance_signal,
    lookup_mapped,
    payload_mapped,
    result_switch,
    forget_dynamic_share,
    additive_forget_logarithm,
    forget_feature_offset,
    substitution_dynamic_share,
    substitution_feature_offset,
    diagonal_reward_scales,
    result_matrix,
    mlp_rescaler,
    switch_matrix,
    expand_matrix,
    contract_matrix,
):
    matrix_length, matrix_breadth = acceptance_signal.shape
    attention_groups = matrix_breadth // PER_GROUP_DIMS
    gate_whole, up_whole, down_whole = (
        lax.all_gather(switch_matrix, "sp", axis=0, tiled=True),
        lax.all_gather(expand_matrix, "sp", axis=0, tiled=True),
        lax.all_gather(contract_matrix, "sp", axis=0, tiled=True),
    )

    def by_head(values):
        return values.astype(jnp.float32).reshape(matrix_length, attention_groups, PER_GROUP_DIMS)

    acceptance_lines = by_head(acceptance_signal)
    lookup_vectors = by_head(lookup_mapped)
    payload_vectors = by_head(payload_mapped)
    log_decay_rate = (
        -jax.nn.softplus(
            -(forget_feature_offset[None, :] + forget_dynamic_share.astype(jnp.float32))
        )
        - 0.5
    )
    log_step = (
        -jnp.exp(log_decay_rate).reshape(matrix_length, attention_groups, PER_GROUP_DIMS)
        + additive_forget_logarithm[:, :, None]
    )
    replace_rate = jax.nn.sigmoid(
        substitution_feature_offset[None, :] + substitution_dynamic_share.astype(jnp.float32)
    )
    replace_rate = replace_rate.reshape(matrix_length, attention_groups, PER_GROUP_DIMS)
    unit_key = lookup_vectors * lax.rsqrt(
        jnp.sum(lookup_vectors * lookup_vectors, axis=-1, keepdims=True) + norm_eps
    )
    block_len = min(64, matrix_length)
    block_count = matrix_length // block_len

    def to_blocks(values):
        return values.reshape(block_count, block_len, attention_groups, PER_GROUP_DIMS).transpose(
            0, 2, 1, 3
        )

    def from_blocks(values):
        return values.transpose(0, 2, 1, 3).reshape(matrix_length, attention_groups, PER_GROUP_DIMS)

    identity_mats = jnp.broadcast_to(
        jnp.eye(PER_GROUP_DIMS, dtype=jnp.float32),
        (attention_groups, PER_GROUP_DIMS, PER_GROUP_DIMS),
    )
    zero_mats = jnp.zeros((attention_groups, PER_GROUP_DIMS, PER_GROUP_DIMS), jnp.float32)
    (closing_state, closing_map), (local_blocks, coef_blocks) = lax.scan(
        block_step,
        (zero_mats, identity_mats),
        (
            to_blocks(acceptance_lines),
            to_blocks(log_step),
            to_blocks(lookup_vectors),
            to_blocks(payload_vectors),
            to_blocks(unit_key),
            to_blocks(replace_rate),
        ),
    )
    _, carried = prefix((closing_map, closing_state), "sp", compose, (identity_mats, zero_mats))
    outcome = from_blocks(local_blocks) + jnp.einsum(
        "hvk,thk->thv", carried, from_blocks(coef_blocks), precision=exact
    )
    centre = jnp.mean(outcome, axis=-1, keepdims=True)
    spread = jnp.mean(jnp.square(outcome - centre), axis=-1, keepdims=True)
    rescaled_attention = (outcome - centre) * lax.rsqrt(spread + group_eps)
    diagonal_reward_summand = (
        jnp.sum(
            acceptance_lines
            * lookup_vectors
            * diagonal_reward_scales.reshape(attention_groups, PER_GROUP_DIMS),
            axis=-1,
            keepdims=True,
        )
        * payload_vectors
    )
    merged_attention = (
        (rescaled_attention + diagonal_reward_summand).reshape(matrix_length, matrix_breadth)
        * result_switch.astype(jnp.float32)
    ).astype(jnp.bfloat16)
    row_block = merged_attention
    projected = lax.psum_scatter(
        jnp.dot(row_block, result_matrix, preferred_element_type=jnp.float32).astype(jnp.bfloat16),
        "tp",
        scatter_dimension=0,
        tiled=True,
    )
    stream = skip_stream.astype(jnp.float32) + lax.optimization_barrier(projected).astype(
        jnp.float32
    )
    scale_rows = lax.rsqrt(jnp.mean(stream * stream, axis=-1, keepdims=True) + norm_eps)
    normed_rows = (stream * scale_rows * mlp_rescaler[None, :]).astype(jnp.bfloat16)
    whole_rows = lax.all_gather(normed_rows, "tp", axis=0, tiled=True)
    gate_act = jnp.dot(whole_rows, gate_whole, preferred_element_type=jnp.float32)
    up_act = jnp.dot(whole_rows, up_whole, preferred_element_type=jnp.float32)
    hidden = (jax.nn.silu(gate_act) * up_act).astype(jnp.bfloat16)
    row_block = hidden
    ffn_out = lax.psum_scatter(
        lax.dot_general(
            row_block, down_whole, (((1,), (1,)), ((), ())), preferred_element_type=jnp.float32
        ).astype(jnp.bfloat16),
        "tp",
        scatter_dimension=0,
        tiled=True,
    )
    return (stream + half_step * lax.optimization_barrier(ffn_out).astype(jnp.float32)).astype(
        jnp.bfloat16
    )


def solution(mesh):
    placed = (
        P(("sp", "tp"), None),
        P("sp", "tp"),
        P("sp", "tp"),
        P("sp", "tp"),
        P("sp", "tp"),
        P("sp", "tp"),
        P("sp", "tp"),
        P("tp"),
        P("sp", "tp"),
        P("tp"),
        P("tp"),
        P("tp", None),
        P(),
        P("sp", "tp"),
        P("sp", "tp"),
        P("sp", "tp"),
    )
    return jax.shard_map(
        per_device, mesh=mesh, in_specs=placed, out_specs=P(("sp", "tp"), None), check_vma=False
    )
```

profile of v0, /device:TPU:0, one launch (start us, length us, event | category | flops | bytes accessed | tf_op | source)
XLA Modules:
  0.0 1402.7 jit_solution(8593175602504717770)
XLA Ops:
  18.0 3.3 reshape_reshape.12
  22.7 3.4 reshape_reshape.13
  28.7 3.4 neg.31
  32.3 3.3 reshape_reshape.15
  38.4 3.4 reshape_reshape.14
  41.8 7.2 multiply_bitcast_fusion
  49.7 873.4 %while.30 = (s32[]{:T(128)}, f32[8,64,64]{2,1,0:T(8,128)}, f32[8,64,64]{1,2,0:T(8,128)}, f32[12,8,64,64]{3,2,1,0:T(8,128)}, f32[12,8,64,64]{3,2,1,0:T(8,128)}, /...) while((s32[]{:T(128)}, f32[8,64,64]{2,1,0:T(8,128)}, ...), condition=%wide.region_3.4_spmd.clone, body=%wide.region_1.3_spmd.clone.sunk | while | flops 431059008 | bytes 15468349 | solution.py:166
  51.5 6.3 fusion.174
  70.3 40.7 %custom-call.9 = f32[8,1,64,64]{2,3,1,0:T(8,128)} custom-call(f32[8,1,64,64]{3,2,1,0:T(8,128)} %fusion.178), custom_call_target="InvertDiagBlocksLowerTriangular" | custom-call | tf_op jit(solution)/shard_map/while/body/eval_jaxpr/jit(_solve_triangular)/vmap()/triangular_solve | solution.py:74
  122.5 6.3 fusion.174
  142.2 40.7 %custom-call.9 = f32[8,1,64,64]{2,3,1,0:T(8,128)} custom-call(f32[8,1,64,64]{3,2,1,0:T(8,128)} %fusion.178), custom_call_target="InvertDiagBlocksLowerTriangular" | custom-call | tf_op jit(solution)/shard_map/while/body/eval_jaxpr/jit(_solve_triangular)/vmap()/triangular_solve | solution.py:74
  195.4 6.3 fusion.174
  215.1 40.7 %custom-call.9 = f32[8,1,64,64]{2,3,1,0:T(8,128)} custom-call(f32[8,1,64,64]{3,2,1,0:T(8,128)} %fusion.178), custom_call_target="InvertDiagBlocksLowerTriangular" | custom-call | tf_op jit(solution)/shard_map/while/body/eval_jaxpr/jit(_solve_triangular)/vmap()/triangular_solve | solution.py:74
  268.4 6.3 fusion.174
  288.1 40.7 %custom-call.9 = f32[8,1,64,64]{2,3,1,0:T(8,128)} custom-call(f32[8,1,64,64]{3,2,1,0:T(8,128)} %fusion.178), custom_call_target="InvertDiagBlocksLowerTriangular" | custom-call | tf_op jit(solution)/shard_map/while/body/eval_jaxpr/jit(_solve_triangular)/vmap()/triangular_solve | solution.py:74
  341.3 6.3 fusion.174
  361.1 40.7 %custom-call.9 = f32[8,1,64,64]{2,3,1,0:T(8,128)} custom-call(f32[8,1,64,64]{3,2,1,0:T(8,128)} %fusion.178), custom_call_target="InvertDiagBlocksLowerTriangular" | custom-call | tf_op jit(solution)/shard_map/while/body/eval_jaxpr/jit(_solve_triangular)/vmap()/triangular_solve | solution.py:74
  414.3 6.3 fusion.174
  434.0 40.7 %custom-call.9 = f32[8,1,64,64]{2,3,1,0:T(8,128)} custom-call(f32[8,1,64,64]{3,2,1,0:T(8,128)} %fusion.178), custom_call_target="InvertDiagBlocksLowerTriangular" | custom-call | tf_op jit(solution)/shard_map/while/body/eval_jaxpr/jit(_solve_triangular)/vmap()/triangular_solve | solution.py:74
  487.2 6.3 fusion.174
  506.9 40.7 %custom-call.9 = f32[8,1,64,64]{2,3,1,0:T(8,128)} custom-call(f32[8,1,64,64]{3,2,1,0:T(8,128)} %fusion.178), custom_call_target="InvertDiagBlocksLowerTriangular" | custom-call | tf_op jit(solution)/shard_map/while/body/eval_jaxpr/jit(_solve_triangular)/vmap()/triangular_solve | solution.py:74
  560.1 6.3 fusion.174
  579.8 40.7 %custom-call.9 = f32[8,1,64,64]{2,3,1,0:T(8,128)} custom-call(f32[8,1,64,64]{3,2,1,0:T(8,128)} %fusion.178), custom_call_target="InvertDiagBlocksLowerTriangular" | custom-call | tf_op jit(solution)/shard_map/while/body/eval_jaxpr/jit(_solve_triangular)/vmap()/triangular_solve | solution.py:74
  633.1 6.3 fusion.174
  652.8 40.7 %custom-call.9 = f32[8,1,64,64]{2,3,1,0:T(8,128)} custom-call(f32[8,1,64,64]{3,2,1,0:T(8,128)} %fusion.178), custom_call_target="InvertDiagBlocksLowerTriangular" | custom-call | tf_op jit(solution)/shard_map/while/body/eval_jaxpr/jit(_solve_triangular)/vmap()/triangular_solve | solution.py:74
  706.0 6.3 fusion.174
  725.7 40.7 %custom-call.9 = f32[8,1,64,64]{2,3,1,0:T(8,128)} custom-call(f32[8,1,64,64]{3,2,1,0:T(8,128)} %fusion.178), custom_call_target="InvertDiagBlocksLowerTriangular" | custom-call | tf_op jit(solution)/shard_map/while/body/eval_jaxpr/jit(_solve_triangular)/vmap()/triangular_solve | solution.py:74
  779.0 6.3 fusion.174
  798.7 40.7 %custom-call.9 = f32[8,1,64,64]{2,3,1,0:T(8,128)} custom-call(f32[8,1,64,64]{3,2,1,0:T(8,128)} %fusion.178), custom_call_target="InvertDiagBlocksLowerTriangular" | custom-call | tf_op jit(solution)/shard_map/while/body/eval_jaxpr/jit(_solve_triangular)/vmap()/triangular_solve | solution.py:74
  851.9 6.3 fusion.174
  871.6 40.7 %custom-call.9 = f32[8,1,64,64]{2,3,1,0:T(8,128)} custom-call(f32[8,1,64,64]{3,2,1,0:T(8,128)} %fusion.178), custom_call_target="InvertDiagBlocksLowerTriangular" | custom-call | tf_op jit(solution)/shard_map/while/body/eval_jaxpr/jit(_solve_triangular)/vmap()/triangular_solve | solution.py:74
  924.2 36.5 %all-gather = bf16[64,64,64]{2,1,0:T(8,128)(2,1)} all-gather(bf16[8,64,64]{2,1,0:T(8,128)(2,1)S(1)} %copy.124), channel_id=2, replica_groups=mesh['sp'=8,'tp'=4] {'sp'}, dimensions={0}, use_global_device_ids=true | all-gather | bytes 589824 | tf_op jit(solution)/shard_map/all_gather | solution.py:18
  960.7 35.2 %all-gather.1 = bf16[64,64,64]{2,1,0:T(8,128)(2,1)} all-gather(bf16[8,64,64]{2,1,0:T(8,128)(2,1)S(1)} %convert_element_type.78), channel_id=3, replica_groups=mesh['sp'=8,'tp'=4] {'sp'}, dimensions={0}, use_global_device_ids=true | all-gather | bytes 589824 | tf_op jit(solution)/shard_map/all_gather | solution.py:18
  996.0 5.4 copy.122
  1001.4 4.5 reshape.78
  1005.9 5.2 copy.123
  1011.1 4.5 reshape.79
  1015.6 3.4 fusion.65
  1020.5 4.0 multiply_add_fusion
  1027.5 4.9 convolution_convert_fusion
  1033.1 54.8 %reduce-scatter.3.cloned.1.call-done = bf16[192,2048]{1,0:T(8,128)(2,1)} async-done(((bf16[768,2048]{1,0:T(8,128)(2,1)}), bf16[192,2048]{1,0:T(8,128)(2,1)}) %reduce-scatter.3.cloned.1.call-update) | async-done | bytes 786448 | tf_op jit(solution)/shard_map/reduce_scatter | solution.py:200
  1092.1 46.1 %all-gather.9.cloned.1.call-done = bf16[2048,1280]{1,0:T(8,128)(2,1)} async-done(((bf16[256,1280]{1,0:T(8,128)(2,1)}), bf16[2048,1280]{1,0:T(8,128)(2,1)}) %all-gather.9.cloned.1.call-update) | async-done | bytes 5242896 | tf_op jit(solution)/shard_map/all_gather | solution.py:122
  1138.2 28.1 %all-gather.7.cloned.1.call-done = bf16[768,2048]{1,0:T(8,128)(2,1)} async-done(((bf16[192,2048]{1,0:T(8,128)(2,1)}), bf16[768,2048]{1,0:T(8,128)(2,1)}) %all-gather.7.cloned.1.call-update) | async-done | bytes 3145744 | tf_op jit(solution)/shard_map/all_gather | solution.py:211
  1166.3 9.5 fusion.66
  1175.9 78.2 %all-gather.11.cloned.1.call-done = bf16[2048,1280]{1,0:T(8,128)(2,1)} async-done(((bf16[256,1280]{1,0:T(8,128)(2,1)}), bf16[2048,1280]{1,0:T(8,128)(2,1)}) %all-gather.11.cloned.1.call-update) | async-done | bytes 5242896 | tf_op jit(solution)/shard_map/all_gather | solution.py:123
  1254.1 86.1 %all-gather.13.cloned.1.call-done = bf16[2048,1280]{1,0:T(8,128)(2,1)} async-done(((bf16[256,1280]{1,0:T(8,128)(2,1)}), bf16[2048,1280]{1,0:T(8,128)(2,1)}) %all-gather.13.cloned.1.call-update) | async-done | bytes 5242896 | tf_op jit(solution)/shard_map/all_gather | solution.py:124
  1340.2 16.0 %convolution_convert_fusion.1 = bf16[768,2048]{1,0:T(8,128)(2,1)} fusion(bf16[2048,1280]{1,0:T(8,128)(2,1)} %all-gather.13.cloned.1.call-done, bf16[768,2048]{1,0:T(8,128)(2,1)} %all-gather.7.cloned.1.call-done, bf16[2048,1280]{1,0:T(8,128)(2,1)} %all-gather.11.cloned.1.call-done, f32[768,1280]{1,0:T(8,128)} %fusion.66), kind=kOutput, calls=%fused_computation.89 | convolution fusion | flops 8060534784 | bytes 20709376 | tf_op jit(solution)/shard_map/dot_general | solution.py:217
  1356.2 36.3 %reduce-scatter.5.cloned.1.call-done = bf16[192,2048]{1,0:T(8,128)(2,1)} async-done(((bf16[768,2048]{1,0:T(8,128)(2,1)}), bf16[192,2048]{1,0:T(8,128)(2,1)}) %reduce-scatter.5.cloned.1.call-update) | async-done | bytes 786448 | tf_op jit(solution)/shard_map/reduce_scatter | solution.py:216
  (548 shorter events, 339.4 us)
Async XLA Ops:
  7.4 1020.2 %copy-start = (bf16[512,2048]{1,0:T(8,128)(2,1)S(1)}, bf16[512,2048]{1,0:T(8,128)(2,1)}, u32[]{:S(2)}) copy-start(bf16[512,2048]{1,0:T(8,128)(2,1)} %param.31) | copy-start | bytes 6291460
  7.4 1080.6 %reduce-scatter.3.cloned.1.call-start = ((), (), s32[]{:S(2)}) async-start(), calls=%async_computation.2 | async-start | bytes 3932160 | tf_op jit(solution)/shard_map/reduce_scatter | solution.py:200
  18.0 3.3 copy-start.11
  22.7 3.6 copy-start.12
  22.7 3.6 copy-start.16
  28.7 3.4 copy-start.13
  32.3 3.4 copy-start.17
  113.4 3.1 copy-start.7
  116.0 2.9 copy-start.2
  183.5 2.9 copy-start.4
  183.5 2.9 copy-start.5
  186.4 3.1 copy-start.7
  189.0 2.9 copy-start.2
  256.4 2.9 copy-start.4
  256.5 2.9 copy-start.5
  259.3 3.1 copy-start.7
  261.9 2.9 copy-start.2
  329.4 2.9 copy-start.4
  329.4 2.9 copy-start.5
  332.3 3.1 copy-start.7
  334.9 2.9 copy-start.2
  405.2 3.1 copy-start.7
  407.8 2.9 copy-start.2
  478.1 3.1 copy-start.7
  480.7 2.9 copy-start.2
  551.1 3.1 copy-start.7
  553.7 2.9 copy-start.2
  624.0 3.1 copy-start.7
  626.6 2.9 copy-start.2
  694.1 2.9 copy-start.4
  694.1 2.9 copy-start.5
  697.0 3.1 copy-start.7
  699.6 2.9 copy-start.2
  769.9 3.1 copy-start.7
  772.5 2.9 copy-start.2
  842.9 3.1 copy-start.7
  845.4 2.9 copy-start.2
  915.8 3.1 copy-start.7
  918.4 2.9 copy-start.2
  923.1 37.6 %copy-start.3 = (f32[8,64,64]{2,1,0:T(8,128)S(1)}, f32[8,64,64]{2,1,0:T(8,128)}, u32[]{:S(2)}) copy-start(f32[8,64,64]{2,1,0:T(8,128)} %get-tuple-element.112) | copy-start | bytes 393220
  1024.4 3.1 copy-start.18
  1032.4 55.5 %copy-start.8 = (bf16[192,2048]{1,0:T(8,128)(2,1)S(1)}, bf16[192,2048]{1,0:T(8,128)(2,1)}, u32[]{:S(2)}) copy-start(bf16[192,2048]{1,0:T(8,128)(2,1)} %param.20) | copy-start | bytes 2359300
  1032.5 57.0 %copy-start.14 = (f32[2048]{0:T(1024)S(1)}, f32[2048]{0:T(1024)}, u32[]{:S(2)}) copy-start(f32[2048]{0:T(1024)} %param.32) | copy-start | bytes 24580
  1032.5 105.8 %all-gather.9.cloned.1.call-start = ((), (), s32[]{:S(2)}) async-start(), calls=%async_computation.4 | async-start | bytes 5898240 | tf_op jit(solution)/shard_map/all_gather | solution.py:122
  1033.0 133.3 %all-gather.7.cloned.1.call-start = ((), (), s32[]{:S(2)}) async-start(), calls=%async_computation.3 | async-start | bytes 3932160 | tf_op jit(solution)/shard_map/all_gather | solution.py:211
  1090.8 163.3 %all-gather.11.cloned.1.call-start = ((), (), s32[]{:S(2)}) async-start(), calls=%async_computation.5 | async-start | bytes 5898240 | tf_op jit(solution)/shard_map/all_gather | solution.py:123
  1091.3 248.8 %all-gather.13.cloned.1.call-start = ((), (), s32[]{:S(2)}) async-start(), calls=%async_computation.6 | async-start | bytes 5898240 | tf_op jit(solution)/shard_map/all_gather | solution.py:124
  1092.1 300.4 %reduce-scatter.5.cloned.1.call-start = ((), (), s32[]{:S(2)}) async-start(), calls=%async_computation.7 | async-start | bytes 3932160 | tf_op jit(solution)/shard_map/reduce_scatter | solution.py:216
  (43 other events, 105.7 us)
Sparse Core Ops, SparseCore 0:
  1032.6 55.3 reduce-scatter.2
  1356.3 36.1 reduce-scatter.4
Sparse Core Ops, SparseCore 1:
  1035.1 103.0 all-gather.8
  1139.7 26.6 all-gather.6
  1168.4 85.6 all-gather.10
  1256.3 83.9 all-gather.12
where the time goes:
time: 1410 us; the launch traced here: 1400 us
  other arithmetic  601 us (43%)
  waiting for transfers between devices  331 us (23%)
  matrix products  251 us (18%)
  local copies, waits for them, and re-layouts  131 us (9%)
  blocking collectives  71.7 us (5%)
  between operations  15.3 us (1%)
    another operation x36, other arithmetic, block_step(): jax.scipy.linalg.solve_triangular(erase_past, jnp.concatenate([recall_rhs...  488 us
    all_gather x1, waiting for transfers between devices, per_device(): lax.all_gather(contract_matrix, 'sp', axis=0, tiled=True)  86.1 us
    all_gather x1, waiting for transfers between devices, per_device(): lax.all_gather(expand_matrix, 'sp', axis=0, tiled=True)  78.2 us
    another operation x12, other arithmetic, block_step(): cumulate = jnp.cumsum(logstep_blk, axis=1)  75 us
    all_gather x2, blocking collectives, prefix(): lax.all_gather(a.astype(kind), axis)  71.7 us
    dynamic_slice x48, local copies, waits for them, and re-layouts, per_device(): lax.scan(block_step, (zero_mats, identity_mats), (to_blocks(acceptance_li...  68.7 us
    reduce_scatter x1, waiting for transfers between devices, per_device(): lax.psum_scatter(jnp.dot(row_block, result_matrix, preferred_element_type...  54.8 us
    dot_general x48, matrix products, masked_pairs(): jnp.einsum('htc,hjc->htj', left, right, precision=exact)  53.6 us
  transfers between devices with their start and end apart: 6, of which 6 were waited for; matrix products, arithmetic and copies ran while one was open for 1% of the time, Pallas kernels for 0%

commit v1 on v0

v1 whole, which is shorter than its diff:
```python
import functools

import jax
import jax.numpy as jnp
from jax import lax
from jax.experimental import pallas as pl
from jax.experimental.pallas import tpu as pltpu
from jax.sharding import PartitionSpec as P

PER_GROUP_DIMS = 64
PAIR = 2 * PER_GROUP_DIMS

norm_eps = 1e-06
group_eps = 0.00064
half_step = 0.5
exact = lax.Precision.HIGHEST
root_scale = 0.6065306597126334


def mm(left, right, dims=((1,), (0,))):
    return lax.dot_general(
        left.astype(jnp.bfloat16),
        right.astype(jnp.bfloat16),
        (dims, ((), ())),
        preferred_element_type=jnp.float32,
    )


def mm_exact(left, right):
    return lax.dot_general(
        left, right, (((1,), (0,)), ((), ())), precision=exact, preferred_element_type=jnp.float32
    )


def sigmoid(x):
    return 1.0 / (1.0 + jnp.exp(-x))


def lanes_of_first(width):
    lane = lax.broadcasted_iota(jnp.int32, (1, width), 1)
    return (lane & (PAIR - 1)) < PER_GROUP_DIMS


def spread(values):
    first = lanes_of_first(values.shape[1])
    zero = jnp.zeros_like(values)
    return jnp.concatenate([jnp.where(first, values, zero), jnp.where(first, zero, values)], axis=0)


def fold(values):
    half = values.shape[0] // 2
    return values[:half] + values[half:]


def head_ones(scale):
    row = lax.broadcasted_iota(jnp.int32, (PAIR, PAIR), 0)
    col = lax.broadcasted_iota(jnp.int32, (PAIR, PAIR), 1)
    return jnp.where((row < PER_GROUP_DIMS) == (col < PER_GROUP_DIMS), scale, 0.0).astype(jnp.float32)


def scan_kernel(
    read_ref, key_ref, value_ref, forget_ref, rate_ref, loss_ref, forget_off_ref, rate_off_ref,
    local_ref, coef_ref, final_ref, carry_ref,
):
    rows, breadth = read_ref.shape
    length = min(PER_GROUP_DIMS, rows)
    pairs = breadth // PAIR
    size = 2 * length
    row = lax.broadcasted_iota(jnp.int32, (size, size), 0)
    col = lax.broadcasted_iota(jnp.int32, (size, size), 1)
    krow = lax.broadcasted_iota(jnp.int32, (PAIR, PAIR), 0)
    kcol = lax.broadcasted_iota(jnp.int32, (PAIR, PAIR), 1)
    eye_k = krow == kcol
    eye = row == col

    for p in range(pairs):
        carry_ref[p, :, :PAIR] = jnp.zeros((PAIR, PAIR), jnp.float32)
        carry_ref[p, :, PAIR:] = jnp.where(eye_k, 1.0, 0.0).astype(jnp.float32)

    strict = col < row
    inclusive = col <= row
    trow = lax.broadcasted_iota(jnp.int32, (length, length), 0)
    tcol = lax.broadcasted_iota(jnp.int32, (length, length), 1)
    lower = jnp.where(tcol <= trow, 1.0, 0.0).astype(jnp.float32)
    ones = head_ones(1.0)
    first = lanes_of_first(PAIR)
    level_masks = []
    b = 1
    while b < length:
        level_masks.append(
            ((row ^ col) < 2 * b) & ((row & b) != 0) & ((col & b) == 0)
        )
        b *= 2

    P_ = range(pairs)

    def prepare(p, now):
        at = slice(p * PAIR, (p + 1) * PAIR)
        key = key_ref[now, at].astype(jnp.float32)
        read = read_ref[now, at].astype(jnp.float32)
        loss = jnp.where(first, loss_ref[now, 2 * p : 2 * p + 1], loss_ref[now, 2 * p + 1 : 2 * p + 2])
        logstep = loss - root_scale * sigmoid(
            forget_off_ref[:, at] + forget_ref[now, at].astype(jnp.float32)
        )
        rate = sigmoid(rate_off_ref[:, at] + rate_ref[now, at].astype(jnp.float32))
        unit = key * lax.rsqrt(mm_exact(key * key, ones) + norm_eps)
        cum = mm_exact(lower, logstep)
        middle = cum[length // 2 - 1 : length // 2, :]
        last = cum[length - 1 : length, :]
        grow = jnp.exp(cum - middle)
        shrink = jnp.exp(middle - cum)
        before = jnp.exp(cum - logstep - middle) * unit
        from_middle = jnp.exp(middle)
        to_end = jnp.exp(last - middle)
        key_back = key * shrink
        erase_back = unit * rate * shrink
        read_fwd = read * grow
        bf = lambda a: spread(a.astype(jnp.bfloat16))
        end_col = jnp.sum(jnp.where(eye_k, jnp.exp(last), 0.0), axis=1, keepdims=True)
        return dict(
            left=jnp.concatenate([bf(before), bf(read_fwd)], axis=0),
            right=jnp.concatenate([bf(key_back), bf(erase_back)], axis=0),
            start=jnp.concatenate([bf(before * from_middle), bf(read_fwd * from_middle)], axis=0),
            ends=jnp.concatenate([bf(key_back * to_end), bf(-(erase_back * to_end))], axis=0),
            value=spread(value_ref[now, at]),
            end_col=end_col,
        )

    def one_block(turn, _):
        now = pl.ds(turn * length, length)
        prep = [prepare(p, now) for p in P_]
        grams = [mm(d["left"], d["right"], ((1,), (1,))) for d in prep]
        erase = [jnp.where(strict, g[:size, size:], 0.0) for g in grams]
        inverse = [jnp.where(eye, 1.0, jnp.where(level_masks[0], -a, 0.0)) for a in erase]
        for mask in level_masks[1:]:
            part = [mm(jnp.where(mask, a, 0.0), x) for a, x in zip(erase, inverse)]
            inverse = [x - mm(x, y) for x, y in zip(inverse, part)]
        within = [
            mm(
                jnp.concatenate(
                    [jnp.where(strict, g[:size, :size], 0.0), jnp.where(inclusive, g[size:, :size], 0.0)],
                    axis=0,
                ),
                d["value"],
            )
            for g, d in zip(grams, prep)
        ]
        erase_read = [jnp.where(inclusive, g[size:, size:], 0.0) for g in grams]
        carry = [carry_ref[p] for p in P_]
        from_state = [mm(d["start"], z) for d, z in zip(prep, carry)]
        pad = lambda a: jnp.concatenate([a, jnp.zeros_like(a)], axis=1)
        recalled = [
            mm(x, f[:size] + pad(w[:size])) for x, f, w in zip(inverse, from_state, within)
        ]
        outs = [
            f[size:] + pad(w[size:]) - mm(e, r)
            for f, w, e, r in zip(from_state, within, erase_read, recalled)
        ]
        for p in P_:
            d = prep[p]
            stacked = jnp.concatenate(
                [pad(d["value"]), recalled[p].astype(jnp.bfloat16)], axis=0
            )
            carry_ref[p] = d["end_col"] * carry[p] + mm(d["ends"], stacked, ((0,), (0,)))
            out = fold(outs[p])
            at = slice(p * PAIR, (p + 1) * PAIR)
            local_ref[now, at] = out[:, :PAIR]
            coef_ref[now, at] = out[:, PAIR:].astype(coef_ref.dtype)
        return 0

    lax.fori_loop(0, rows // length, one_block, 0)
    for p in P_:
        final_ref[p] = fold(carry_ref[p])


def local_scan(read, key, value, forget, rate, loss, forget_off, rate_off):
    rows, breadth = read.shape
    pairs = breadth // PAIR
    return pl.pallas_call(
        scan_kernel,
        out_shape=[
            jax.ShapeDtypeStruct((rows, breadth), jnp.float32),
            jax.ShapeDtypeStruct((rows, breadth), jnp.bfloat16),
            jax.ShapeDtypeStruct((pairs, PER_GROUP_DIMS, 2 * PAIR), jnp.float32),
        ],
        scratch_shapes=[pltpu.VMEM((pairs, PAIR, 2 * PAIR), jnp.float32)],
        name="local_scan",
    )(read, key, value, forget, rate, loss, forget_off[None, :], rate_off[None, :])


def join_kernel(earlier_ref, later_ref, out_ref, sent_ref):
    for p in range(later_ref.shape[0]):
        later = later_ref[p]
        moved = mm(spread(later[:, PAIR:]), spread(earlier_ref[p]))
        total = fold(moved) + jnp.concatenate(
            [later[:, :PAIR], jnp.zeros_like(later[:, :PAIR])], axis=1
        )
        out_ref[p] = total
        sent_ref[p] = total.astype(sent_ref.dtype)


def prefix(own, axis, count):
    def shifted(values, by):
        return lax.ppermute(values, axis, [(i, i + by) for i in range(count - by)])

    sent = shifted(own.astype(jnp.bfloat16), 1)
    held = sent.astype(jnp.float32)
    by = 1
    while by < count - 1:
        held, sent = pl.pallas_call(
            join_kernel,
            out_shape=[
                jax.ShapeDtypeStruct(own.shape, jnp.float32),
                jax.ShapeDtypeStruct(own.shape, jnp.bfloat16),
            ],
            name="join",
        )(shifted(sent, by), held)
        by *= 2
    return held


def finish_kernel(
    local_ref, coef_ref, carried_ref, read_ref, key_ref, value_ref, gate_ref, reward_ref, out_ref
):
    mean_of = head_ones(1.0 / PER_GROUP_DIMS)
    sum_of = head_ones(1.0)
    for p in range(local_ref.shape[1] // PAIR):
        at = slice(p * PAIR, (p + 1) * PAIR)
        outcome = local_ref[:, at] + mm(coef_ref[:, at], spread(carried_ref[p][:, :PAIR]))
        centred = outcome - mm_exact(outcome, mean_of)
        variance = mm_exact(centred * centred, mean_of)
        normed = centred * lax.rsqrt(variance + group_eps)
        reads = read_ref[:, at].astype(jnp.float32) * key_ref[:, at].astype(jnp.float32)
        bonus = mm_exact(reads * reward_ref[:, at], sum_of) * value_ref[:, at].astype(jnp.float32)
        out_ref[:, at] = ((normed + bonus) * gate_ref[:, at].astype(jnp.float32)).astype(out_ref.dtype)


def finish(local, coef, carried, read, key, value, gate, reward):
    rows, breadth = local.shape
    block = min(128, rows)
    wide = pl.BlockSpec((block, breadth), lambda i: (i, 0))
    return pl.pallas_call(
        finish_kernel,
        grid=(rows // block,),
        in_specs=[wide, wide, pl.BlockSpec(carried.shape, lambda i: (0, 0, 0))]
        + [wide] * 4
        + [pl.BlockSpec((1, breadth), lambda i: (0, 0))],
        out_specs=wide,
        out_shape=jax.ShapeDtypeStruct((rows, breadth), jnp.bfloat16),
        name="finish",
    )(local, coef, carried, read, key, value, gate, reward[None, :])


def per_device(
    sp_count,
    skip_stream,
    acceptance_signal,
    lookup_mapped,
    payload_mapped,
    result_switch,
    forget_dynamic_share,
    additive_forget_logarithm,
    forget_feature_offset,
    substitution_dynamic_share,
    substitution_feature_offset,
    diagonal_reward_scales,
    result_matrix,
    mlp_rescaler,
    switch_matrix,
    expand_matrix,
    contract_matrix,
):
    gate_whole, up_whole, down_whole = (
        lax.all_gather(switch_matrix, "sp", axis=0, tiled=True),
        lax.all_gather(expand_matrix, "sp", axis=0, tiled=True),
        lax.all_gather(contract_matrix, "sp", axis=0, tiled=True),
    )

    local, coef, final = local_scan(
        acceptance_signal,
        lookup_mapped,
        payload_mapped,
        forget_dynamic_share,
        substitution_dynamic_share,
        additive_forget_logarithm,
        forget_feature_offset,
        substitution_feature_offset,
    )
    carried = prefix(final, "sp", sp_count)
    local, gate_whole = lax.optimization_barrier((local, gate_whole))
    merged_attention = finish(
        local,
        coef,
        carried,
        acceptance_signal,
        lookup_mapped,
        payload_mapped,
        result_switch,
        diagonal_reward_scales,
    )
    row_block = merged_attention
    projected = lax.psum_scatter(
        jnp.dot(row_block, result_matrix, preferred_element_type=jnp.float32).astype(jnp.bfloat16),
        "tp",
        scatter_dimension=0,
        tiled=True,
    )
    stream = skip_stream.astype(jnp.float32) + lax.optimization_barrier(projected).astype(
        jnp.float32
    )
    scale_rows = lax.rsqrt(jnp.mean(stream * stream, axis=-1, keepdims=True) + norm_eps)
    normed_rows = (stream * scale_rows * mlp_rescaler[None, :]).astype(jnp.bfloat16)
    whole_rows = lax.all_gather(normed_rows, "tp", axis=0, tiled=True)
    gate_act = jnp.dot(whole_rows, gate_whole, preferred_element_type=jnp.float32)
    up_act = jnp.dot(whole_rows, up_whole, preferred_element_type=jnp.float32)
    hidden = (jax.nn.silu(gate_act) * up_act).astype(jnp.bfloat16)
    row_block = hidden
    ffn_out = lax.psum_scatter(
        lax.dot_general(
            row_block, down_whole, (((1,), (1,)), ((), ())), preferred_element_type=jnp.float32
        ).astype(jnp.bfloat16),
        "tp",
        scatter_dimension=0,
        tiled=True,
    )
    return (stream + half_step * lax.optimization_barrier(ffn_out).astype(jnp.float32)).astype(
        jnp.bfloat16
    )


def solution(mesh):
    placed = (
        P(("sp", "tp"), None),
        P("sp", "tp"),
        P("sp", "tp"),
        P("sp", "tp"),
        P("sp", "tp"),
        P("sp", "tp"),
        P("sp", "tp"),
        P("tp"),
        P("sp", "tp"),
        P("tp"),
        P("tp"),
        P("tp", None),
        P(),
        P("sp", "tp"),
        P("sp", "tp"),
        P("sp", "tp"),
    )
    return jax.shard_map(
        functools.partial(per_device, mesh.shape["sp"]), mesh=mesh, in_specs=placed, out_specs=P(("sp", "tp"), None), check_vma=False
    )
```

time: 1410 us -> 436 us (0.31)
  other arithmetic: 601 us -> 8.12 us
  matrix products: 251 us -> 30.1 us
  local copies, waits for them, and re-layouts: 131 us -> 3.59 us
  blocking collectives: 71.7 us -> 0 us
  Pallas kernels: 0 us -> 55.3 us
  waiting for transfers between devices: 331 us -> 291 us
  starting transfers between devices: 0.21 us -> 34.2 us
    another operation x50 -> x0, other arithmetic: 563 us -> none  [the longest x36 488 us: block_step(): jax.scipy.linalg.solve_triangular(erase_past, jnp.concatenate([recall_rhs...]
    dot_general x181 -> x0, matrix products: 212 us -> none  [the longest x48 53.6 us: masked_pairs(): jnp.einsum('htc,hjc->htj', left, right, precision=exact)]
    all_gather x2 -> x0, blocking collectives: 71.7 us -> none  [prefix(): lax.all_gather(a.astype(kind), axis)]
    dynamic_slice x48 -> x0, local copies, waits for them, and re-layouts: 68.7 us -> none  [per_device(): lax.scan(block_step, (zero_mats, identity_mats), (to_blocks(acceptance_li...]
    pallas_call x0 -> x5, Pallas kernels: none -> 55.3 us  [the longest x1 35.5 us: local_scan(): pl.pallas_call(scan_kernel, out_shape=[jax.ShapeDtypeStruct((rows, breadt...]
    all_gather x1, waiting for transfers between devices: 46.1 us -> 0.01 us  [per_device(): lax.all_gather(switch_matrix, 'sp', axis=0, tiled=True)]
    ppermute x0 -> x4, starting transfers between devices: none -> 33.8 us  [shifted(): return lax.ppermute(values, axis, [(i, i + by) for i in range(count - by)])]
    ppermute x0 -> x4, waiting for transfers between devices: none -> 20.3 us  [shifted(): return lax.ppermute(values, axis, [(i, i + by) for i in range(count - by)])]
  transfers between devices with their start and end apart: 6 -> 10, of which waited for: 6 -> 9; matrix products, arithmetic and copies ran while one was open for 1% -> 3% of each run, Pallas kernels for 0% -> 10%
where the time goes in v1:
time: 436 us; the launch traced here: 435 us
  waiting for transfers between devices  291 us (67%)
  Pallas kernels  55.3 us (13%)
  starting transfers between devices  34.2 us (8%)
  matrix products  30.1 us (7%)
  between operations  13.5 us (3%)
  other arithmetic  8.12 us (2%)
    all_gather x1, waiting for transfers between devices, per_device(): lax.all_gather(expand_matrix, 'sp', axis=0, tiled=True)  86.1 us
    all_gather x1, waiting for transfers between devices, per_device(): lax.all_gather(contract_matrix, 'sp', axis=0, tiled=True)  78.4 us
    reduce_scatter x1, waiting for transfers between devices, per_device(): lax.psum_scatter(jnp.dot(row_block, result_matrix, preferred_element_type...  40.4 us
    reduce_scatter x1, waiting for transfers between devices, per_device(): lax.psum_scatter(lax.dot_general(row_block, down_whole, (((1,), (1,)), ((...  36.2 us
    pallas_call x1, Pallas kernels, local_scan(): pl.pallas_call(scan_kernel, out_shape=[jax.ShapeDtypeStruct((rows, breadt...  35.5 us
    ppermute x4, starting transfers between devices, shifted(): return lax.ppermute(values, axis, [(i, i + by) for i in range(count - by)])  33.8 us
    all_gather x1, waiting for transfers between devices, per_device(): whole_rows = lax.all_gather(normed_rows, 'tp', axis=0, tiled=True)  27.3 us
    ppermute x4, waiting for transfers between devices, shifted(): return lax.ppermute(values, axis, [(i, i + by) for i in range(count - by)])  20.3 us
  transfers between devices with their start and end apart: 10, of which 9 were waited for; matrix products, arithmetic and copies ran while one was open for 3% of the time, Pallas kernels for 10%

profile of v1, /device:TPU:0, one launch (start us, length us, event | category | flops | bytes accessed | tf_op | source)
XLA Modules:
  0.0 435.4 jit_solution(16967475954001121727)
XLA Ops:
  6.5 0.0 copy-start
  6.5 0.0 all-gather.5.cloned.1.call-start
  6.5 0.7 all-gather.5.cloned.1.call-update
  7.3 0.0 reduce-scatter.3.cloned.1.call-start
  7.3 1.7 copy.17.loss_ref
  9.0 35.5 %local_scan.1 = (f32[768,512]{1,0:T(8,128)}, bf16[768,512]{1,0:T(8,128)(2,1)}, f32[4,64,256]{2,1,0:T(8,128)}) custom-call(bf16[768,512]{1,0:T(8,128)(2,1)} %read_ref.3, bf16[768,512]{1,0:T(8,128)(2,1)} %key_ref.3, bf16[768,512]{1,0:T(8,128)(2,1)} %value_ref.3, bf16[768,512]{1,0:T(8,128)(2,1)} %forget_ref.1, bf16[768,512]{1,0:T(8,128)(2,1)} %rate_ref.1, ...), custom_call_target="tpu_custom_call" | custom-call | tf_op jit(solution)/shard_map/local_scan/pallas_call | solution.py:179
  44.4 1.0 convert_element_type.31
  45.4 4.9 %collective-permute-start = (bf16[4,64,256]{2,1,0:T(8,128)(2,1)S(1)}, bf16[4,64,256]{2,1,0:T(8,128)(2,1)S(1)}, u32[]{:S(2)}, u32[]{:S(2)}) collective-permute-start(bf16[4,64,256]{2,1,0:T(8,128)(2,1)S(1)} %convert_element_type.31), channel_id=1, source_target_pairs={{0,4},{4,8},{8,12},{12,16},{16,20},{20,24},{24,28},{1,5},{5,9},{9,... | collective-permute-start | bytes 393224 | tf_op jit(solution)/shard_map/ppermute | solution.py:204
  50.3 6.2 %collective-permute-done = bf16[4,64,256]{2,1,0:T(8,128)(2,1)S(1)} collective-permute-done((bf16[4,64,256]{2,1,0:T(8,128)(2,1)S(1)}, bf16[4,64,256]{2,1,0:T(8,128)(2,1)S(1)}, u32[]{:S(2)}, u32[]{:S(2)}) %collective-permute-start) | collective-permute-done | bytes 131104 | tf_op jit(solution)/shard_map/ppermute | solution.py:204
  56.6 4.4 %collective-permute-start.1 = (bf16[4,64,256]{2,1,0:T(8,128)(2,1)S(1)}, bf16[4,64,256]{2,1,0:T(8,128)(2,1)S(1)}, u32[]{:S(2)}, u32[]{:S(2)}) collective-permute-start(bf16[4,64,256]{2,1,0:T(8,128)(2,1)S(1)} %collective-permute-done), channel_id=1, source_target_pairs={{0,4},{4,8},{8,12},{12,16},{16,20},{20,24},{24,28},{1,5},{5,9},{9,... | collective-permute-start | bytes 393224 | tf_op jit(solution)/shard_map/ppermute | solution.py:204
  60.9 0.7 convert_element_type.32.later_ref
  61.7 5.3 %collective-permute-done.1.earlier_ref = bf16[4,64,256]{2,1,0:T(8,128)(2,1)S(1)} collective-permute-done((bf16[4,64,256]{2,1,0:T(8,128)(2,1)S(1)}, bf16[4,64,256]{2,1,0:T(8,128)(2,1)S(1)}, u32[]{:S(2)}, u32[]{:S(2)}) %collective-permute-start.1) | collective-permute-done | bytes 131104 | tf_op jit(solution)/shard_map/ppermute | solution.py:204
  67.0 0.0 copy-start.4
  67.0 0.6 copy-done.4
  67.7 2.0 join.3
  69.7 6.0 %collective-permute-start.2 = (bf16[4,64,256]{2,1,0:T(8,128)(2,1)}, bf16[4,64,256]{2,1,0:T(8,128)(2,1)S(1)}, u32[]{:S(2)}, u32[]{:S(2)}) collective-permute-start(bf16[4,64,256]{2,1,0:T(8,128)(2,1)} %get-tuple-element.19), channel_id=1, source_target_pairs={{0,8},{4,12},{8,16},{12,20},{16,24},{20,28},{1,9},{5,13},{9,17},{1... | collective-permute-start | bytes 393224 | tf_op jit(solution)/shard_map/ppermute | solution.py:204
  75.7 5.9 %collective-permute-done.2.earlier_ref = bf16[4,64,256]{2,1,0:T(8,128)(2,1)S(1)} collective-permute-done((bf16[4,64,256]{2,1,0:T(8,128)(2,1)}, bf16[4,64,256]{2,1,0:T(8,128)(2,1)S(1)}, u32[]{:S(2)}, u32[]{:S(2)}) %collective-permute-start.2) | collective-permute-done | bytes 131104 | tf_op jit(solution)/shard_map/ppermute | solution.py:204
  81.6 0.0 copy-start.2
  81.6 0.6 copy-done.2
  82.3 2.0 join.4
  84.3 18.5 %collective-permute-start.3 = (bf16[4,64,256]{2,1,0:T(8,128)(2,1)}, bf16[4,64,256]{2,1,0:T(8,128)(2,1)S(1)}, u32[]{:S(2)}, u32[]{:S(2)}) collective-permute-start(bf16[4,64,256]{2,1,0:T(8,128)(2,1)} %get-tuple-element.21), channel_id=1, source_target_pairs={{0,16},{4,20},{8,24},{12,28},{1,17},{5,21},{9,25},{13,29},{2,18},{... | collective-permute-start | bytes 393224 | tf_op jit(solution)/shard_map/ppermute | solution.py:204
  102.7 2.8 collective-permute-done.3.earlier_ref
  105.6 0.6 copy-done.3
  106.2 2.0 join.5
  108.2 13.8 %finish.1 = bf16[768,512]{1,0:T(8,128)(2,1)} custom-call(f32[768,512]{1,0:T(8,128)} %get-tuple-element.16.local_ref, bf16[768,512]{1,0:T(8,128)(2,1)} %get-tuple-element.17.coef_ref, f32[4,64,256]{2,1,0:T(8,128)} %get-tuple-element.23.carried_ref, bf16[768,512]{1,0:T(8,128)(2,1)} %read_ref.3, bf16[768,512]{1,0:T(8,128)(2,1)} %key_ref.3, ...), custom_call_target="tpu_custom_call" | custom-call | tf_op jit(solution)/shard_map/finish/pallas_call | solution.py:242
  122.0 0.0 copy-done
  122.0 4.6 %convolution_convert_fusion = bf16[768,2048]{1,0:T(8,128)(2,1)} fusion(bf16[768,512]{1,0:T(8,128)(2,1)} %finish.1, bf16[512,2048]{1,0:T(8,128)(2,1)S(1)} %copy-done), kind=kOutput, calls=%fused_computation.1 | convolution fusion | flops 1612185600 | bytes 6029312 | tf_op jit(solution)/shard_map/dot_general | solution.py:303
  126.6 0.0 reduce-scatter.3.cloned.1.call-update
  126.7 0.0 all-gather.7.cloned.1.call-start
  126.7 40.4 %reduce-scatter.3.cloned.1.call-done = bf16[192,2048]{1,0:T(8,128)(2,1)} async-done(((bf16[768,2048]{1,0:T(8,128)(2,1)}), bf16[192,2048]{1,0:T(8,128)(2,1)}) %reduce-scatter.3.cloned.1.call-update) | async-done | bytes 786448 | tf_op jit(solution)/shard_map/reduce_scatter | solution.py:302
  167.1 0.0 copy-done.1
  167.1 1.5 multiply_reduce_fusion
  168.6 0.0 copy-done.5
  168.6 2.3 multiply_convert_fusion
  170.9 0.0 all-gather.7.cloned.1.call-update
  170.9 0.0 all-gather.11.cloned.1.call-start
  171.0 0.5 all-gather.11.cloned.1.call-update
  171.5 0.0 all-gather.9.cloned.1.call-start
  171.5 0.5 all-gather.9.cloned.1.call-update
  172.1 0.2 reduce-scatter.5.cloned.1.call-start
  172.3 27.3 %all-gather.7.cloned.1.call-done = bf16[768,2048]{1,0:T(8,128)(2,1)} async-done(((bf16[192,2048]{1,0:T(8,128)(2,1)}), bf16[768,2048]{1,0:T(8,128)(2,1)}) %all-gather.7.cloned.1.call-update) | async-done | bytes 3145744 | tf_op jit(solution)/shard_map/all_gather | solution.py:313
  199.6 9.5 %fusion.2 = f32[768,1280]{1,0:T(8,128)} fusion(bf16[768,2048]{1,0:T(8,128)(2,1)} %all-gather.7.cloned.1.call-done, bf16[2048,1280]{1,0:T(8,128)(2,1)} %all-gather.5.cloned.1.call-done), kind=kOutput, calls=%fused_computation.10 | convolution fusion | flops 4026531840 | bytes 12320768 | tf_op jit(solution)/shard_map/dot_general | solution.py:314
  209.1 78.4 %all-gather.11.cloned.1.call-done = bf16[2048,1280]{1,0:T(8,128)(2,1)} async-done(((bf16[256,1280]{1,0:T(8,128)(2,1)}), bf16[2048,1280]{1,0:T(8,128)(2,1)}) %all-gather.11.cloned.1.call-update) | async-done | bytes 5242896 | tf_op jit(solution)/shard_map/all_gather | solution.py:276
  287.5 86.1 %all-gather.9.cloned.1.call-done = bf16[2048,1280]{1,0:T(8,128)(2,1)} async-done(((bf16[256,1280]{1,0:T(8,128)(2,1)}), bf16[2048,1280]{1,0:T(8,128)(2,1)}) %all-gather.9.cloned.1.call-update) | async-done | bytes 5242896 | tf_op jit(solution)/shard_map/all_gather | solution.py:275
  373.7 16.0 %convolution_convert_fusion.1 = bf16[768,2048]{1,0:T(8,128)(2,1)} fusion(bf16[2048,1280]{1,0:T(8,128)(2,1)} %all-gather.11.cloned.1.call-done, bf16[768,2048]{1,0:T(8,128)(2,1)} %all-gather.7.cloned.1.call-done, bf16[2048,1280]{1,0:T(8,128)(2,1)} %all-gather.9.cloned.1.call-done, f32[768,1280]{1,0:T(8,128)} %fusion.2), kind=kOutput, calls=%fused_computation.3 | convolution fusion | flops 8060534784 | bytes 20709376 | tf_op jit(solution)/shard_map/dot_general | solution.py:319
  389.6 0.0 reduce-scatter.5.cloned.1.call-update
  389.6 36.2 %reduce-scatter.5.cloned.1.call-done = bf16[192,2048]{1,0:T(8,128)(2,1)} async-done(((bf16[768,2048]{1,0:T(8,128)(2,1)}), bf16[192,2048]{1,0:T(8,128)(2,1)}) %reduce-scatter.5.cloned.1.call-update) | async-done | bytes 786448 | tf_op jit(solution)/shard_map/reduce_scatter | solution.py:318
  425.9 2.7 add_convert_fusion
  (5 shorter events, 0.0 us)
Async XLA Ops:
  6.5 115.5 %copy-start = (bf16[512,2048]{1,0:T(8,128)(2,1)S(1)}, bf16[512,2048]{1,0:T(8,128)(2,1)}, u32[]{:S(2)}) copy-start(bf16[512,2048]{1,0:T(8,128)(2,1)} %param.27) | copy-start | bytes 6291460
  6.5 101.6 %all-gather.5.cloned.1.call-start = ((), (), s32[]{:S(2)}) async-start(), calls=%async_computation.2 | async-start | bytes 5898240 | tf_op jit(solution)/shard_map/all_gather | solution.py:274
  7.3 159.8 %reduce-scatter.3.cloned.1.call-start = ((), (), s32[]{:S(2)}) async-start(), calls=%async_computation.3 | async-start | bytes 3932160 | tf_op jit(solution)/shard_map/reduce_scatter | solution.py:302
  45.4 11.1 %collective-permute-start = (bf16[4,64,256]{2,1,0:T(8,128)(2,1)S(1)}, bf16[4,64,256]{2,1,0:T(8,128)(2,1)S(1)}, u32[]{:S(2)}, u32[]{:S(2)}) collective-permute-start(bf16[4,64,256]{2,1,0:T(8,128)(2,1)S(1)} %convert_element_type.31), channel_id=1, source_target_pairs={{0,4},{4,8},{8,12},{12,16},{16,20},{20,24},{24,28},{1,5},{5,9},{9,... | collective-permute-start | bytes 393224 | tf_op jit(solution)/shard_map/ppermute | solution.py:204
  56.6 10.5 %collective-permute-start.1 = (bf16[4,64,256]{2,1,0:T(8,128)(2,1)S(1)}, bf16[4,64,256]{2,1,0:T(8,128)(2,1)S(1)}, u32[]{:S(2)}, u32[]{:S(2)}) collective-permute-start(bf16[4,64,256]{2,1,0:T(8,128)(2,1)S(1)} %collective-permute-done), channel_id=1, source_target_pairs={{0,4},{4,8},{8,12},{12,16},{16,20},{20,24},{24,28},{1,5},{5,9},{9,... | collective-permute-start | bytes 393224 | tf_op jit(solution)/shard_map/ppermute | solution.py:204
  67.0 0.6 copy-start.4
  69.7 12.0 %collective-permute-start.2 = (bf16[4,64,256]{2,1,0:T(8,128)(2,1)}, bf16[4,64,256]{2,1,0:T(8,128)(2,1)S(1)}, u32[]{:S(2)}, u32[]{:S(2)}) collective-permute-start(bf16[4,64,256]{2,1,0:T(8,128)(2,1)} %get-tuple-element.19), channel_id=1, source_target_pairs={{0,8},{4,12},{8,16},{12,20},{16,24},{20,28},{1,9},{5,13},{9,17},{1... | collective-permute-start | bytes 393224 | tf_op jit(solution)/shard_map/ppermute | solution.py:204
  81.6 0.6 copy-start.2
  84.3 21.3 %collective-permute-start.3 = (bf16[4,64,256]{2,1,0:T(8,128)(2,1)}, bf16[4,64,256]{2,1,0:T(8,128)(2,1)S(1)}, u32[]{:S(2)}, u32[]{:S(2)}) collective-permute-start(bf16[4,64,256]{2,1,0:T(8,128)(2,1)} %get-tuple-element.21), channel_id=1, source_target_pairs={{0,16},{4,20},{8,24},{12,28},{1,17},{5,21},{9,25},{13,29},{2,18},{... | collective-permute-start | bytes 393224 | tf_op jit(solution)/shard_map/ppermute | solution.py:204
  105.6 0.6 copy-start.3
  126.6 40.5 %copy-start.1 = (bf16[192,2048]{1,0:T(8,128)(2,1)S(1)}, bf16[192,2048]{1,0:T(8,128)(2,1)}, u32[]{:S(2)}) copy-start(bf16[192,2048]{1,0:T(8,128)(2,1)} %param.16) | copy-start | bytes 2359300
  126.6 41.9 %copy-start.5 = (f32[2048]{0:T(1024)S(1)}, f32[2048]{0:T(1024)}, u32[]{:S(2)}) copy-start(f32[2048]{0:T(1024)} %param.28) | copy-start | bytes 24580
  126.7 72.9 %all-gather.7.cloned.1.call-start = ((), (), s32[]{:S(2)}) async-start(), calls=%async_computation.4 | async-start | bytes 3932160 | tf_op jit(solution)/shard_map/all_gather | solution.py:313
  170.9 116.6 %all-gather.11.cloned.1.call-start = ((), (), s32[]{:S(2)}) async-start(), calls=%async_computation.6 | async-start | bytes 5898240 | tf_op jit(solution)/shard_map/all_gather | solution.py:276
  171.5 202.2 %all-gather.9.cloned.1.call-start = ((), (), s32[]{:S(2)}) async-start(), calls=%async_computation.5 | async-start | bytes 5898240 | tf_op jit(solution)/shard_map/all_gather | solution.py:275
  172.1 253.8 %reduce-scatter.5.cloned.1.call-start = ((), (), s32[]{:S(2)}) async-start(), calls=%async_computation.7 | async-start | bytes 3932160 | tf_op jit(solution)/shard_map/reduce_scatter | solution.py:318
Sparse Core Ops, SparseCore 0:
  9.5 94.4 all-gather.4
  126.8 40.2 reduce-scatter.2
  171.0 28.4 all-gather.6
  201.6 85.8 all-gather.10
  289.6 84.0 all-gather.8
  389.8 36.0 reduce-scatter.4
